TPU v7x, 32 devices: a whole 2x2x4 slice. The times are simulated.
32 devices in a mesh: grp: 2 (over y), fs: 4 (over z), tp: 4 (over x, core).
Axes of the slice: x: 2, y: 2, z: 4, core: 2. Of those that a mesh axis runs over, the one named last changes fastest.
Arguments:
- tokens: bfloat16 [2560, 2048], P(('grp', 'fs', 'tp')), parts along dimension 0, may hold values from -6 to 6
- mix_gain: bfloat16 [2048], replicated, may hold values from 0.099609375 to 1.8984375
- val_weight: bfloat16 [2048, 1024], P('fs', 'tp'), may hold values from -4 to 4
- gate_weight: bfloat16 [2048, 1024], P('fs', 'tp'), may hold values from -0.125 to 0.125
- conv_taps: bfloat16 [31, 1024], replicated, may hold values from -1 to 1
- chan_gain: bfloat16 [1024], replicated, may hold values from 0.099609375 to 1.8984375
- out_weight: bfloat16 [1024, 2048], P('tp', 'fs'), may hold values from -0.1875 to 0.1875
- mix_post_gain: bfloat16 [2048], replicated, may hold values from 0.099609375 to 1.8984375
- ffn_gain: bfloat16 [2048], replicated, may hold values from 0.099609375 to 1.8984375
- up_gate_weight: bfloat16 [2048, 5120], P('fs', 'tp'), may hold values from -0.125 to 0.125
- up_val_weight: bfloat16 [2048, 5120], P('fs', 'tp'), may hold values from -0.125 to 0.125
- ffn_taps: bfloat16 [2, 3, 5120], replicated, may hold values from -3.5 to 3.5
- down_weight: bfloat16 [5120, 2048], P('tp', 'fs'), may hold values from -0.078125 to 0.078125
- ffn_post_gain: bfloat16 [2048], replicated, may hold values from 0.099609375 to 1.8984375
Outputs:
- layer_out: bfloat16 [2560, 2048], P(('grp', 'fs', 'tp')), parts along dimension 0
There are 2 independent parts, one for each index of `grp`. A program takes and returns all parts, laid end to end along the dimension named above; an argument that names none is the same for every part. Nothing has to cross between parts.
All inputs are finite; a program needn't handle non-finite values.
Results may differ from a plain program's by a relative error of at most 0.019.
Values may be sent and summed in bfloat16 or wider, within the bound.
A program may use at most 64 MiB of HBM per device.

v0:
```python
import functools

import jax
import jax.numpy as jnp
from jax import lax
from jax.experimental import pallas as pl
from jax.experimental.pallas import tpu as pltpu
from jax.sharding import PartitionSpec as P

LEN = 64
LANES = 128
F32 = jnp.float32
BF16 = jnp.bfloat16

norm_epsilon = 1e-06
chan_epsilon = 1e-05


def rms_scale(values, gain):
    inverse = lax.rsqrt(jnp.mean(values * values, axis=-1, keepdims=True) + norm_epsilon)
    return values * inverse * gain.astype(F32)


def depthwise(signal, tap_table):
    taps_count = tap_table.shape[0]
    channels = signal.shape[1]
    shaped = signal.astype(F32).reshape(signal.shape[0] // LEN, LEN, channels)
    padded = jnp.pad(shaped, ((0, 0), (taps_count - 1, 0), (0, 0)))
    tap_values = tap_table.astype(F32)
    result = jnp.zeros(shaped.shape, F32)
    for offset in range(taps_count):
        result = result + padded[:, offset : offset + LEN, :] * tap_values[offset]
    return result.reshape(signal.shape[0], channels)


def gather_rows(weight):
    return lax.all_gather(weight, "fs", axis=0, tiled=True)


def gather_columns(weight):
    return lax.all_gather(weight, "fs", axis=1, tiled=True)


def product(left, right):
    return jnp.dot(left, right, preferred_element_type=F32)


def scatter_sum(part):
    return lax.psum_scatter(
        part.astype(BF16), "tp", scatter_dimension=0, tiled=True
    ).astype(F32)


def plain(
    tokens,
    mix_gain,
    val_weight,
    gate_weight,
    conv_taps,
    chan_gain,
    out_weight,
    mix_post_gain,
    ffn_gain,
    up_gate_weight,
    up_val_weight,
    ffn_taps,
    down_weight,
    ffn_post_gain,
):
    member = lax.axis_index("tp")
    normed_own = rms_scale(tokens.astype(F32), mix_gain).astype(BF16)
    normed = lax.all_gather(normed_own, "tp", axis=0, tiled=True)
    local_ch = val_weight.shape[1]
    values = product(normed, gather_rows(val_weight))
    gate_sums = product(normed, gather_rows(gate_weight))
    glu_out = (values * jax.nn.sigmoid(gate_sums)).astype(BF16)
    own_taps = lax.dynamic_slice_in_dim(conv_taps, member * local_ch, local_ch, 1)
    conv_out = depthwise(glu_out, own_taps)
    totals, squares = lax.psum(
        (jnp.sum(conv_out, axis=1), jnp.sum(conv_out * conv_out, axis=1)), "tp"
    )
    all_channels = chan_gain.shape[0]
    chan_mean = totals[:, None] / all_channels
    chan_var = squares[:, None] / all_channels - chan_mean * chan_mean
    own_gain = lax.dynamic_slice_in_dim(chan_gain, member * local_ch, local_ch, 0).astype(F32)
    activated = jax.nn.silu((conv_out - chan_mean) * lax.rsqrt(chan_var + chan_epsilon) * own_gain)
    mixed_sum = scatter_sum(product(activated.astype(BF16), gather_columns(out_weight)))
    residual = (tokens.astype(F32) + rms_scale(mixed_sum, mix_post_gain)).astype(BF16)
    normed_share = rms_scale(residual.astype(F32), ffn_gain).astype(BF16)
    normed_ffn = lax.all_gather(normed_share, "tp", axis=0, tiled=True)
    local_ff = up_gate_weight.shape[1]
    own_ffn_taps = lax.dynamic_slice_in_dim(ffn_taps, member * local_ff, local_ff, 2)
    up_gate = product(normed_ffn, gather_rows(up_gate_weight)).astype(BF16)
    up_val = product(normed_ffn, gather_rows(up_val_weight)).astype(BF16)
    gate_conv = depthwise(up_gate, own_ffn_taps[0])
    val_conv = depthwise(up_val, own_ffn_taps[1])
    hidden = (jax.nn.gelu(gate_conv, approximate=True) * val_conv).astype(BF16)
    ffn_sum = scatter_sum(product(hidden, gather_columns(down_weight)))
    return (residual.astype(F32) + rms_scale(ffn_sum, ffn_post_gain)).astype(BF16)


def rows_at(start, size, unit=16):
    return pl.ds(pl.multiple_of(start, unit), size)


class Where:
    def __init__(self):
        self.place = lax.axis_index("fs")
        self.half = lax.axis_index("grp")
        self.member = lax.axis_index("tp")
        place, member = self.place, self.member
        self.side = place // 2
        self.inner = jnp.logical_or(place == 1, place == 2)
        self.chip = member // 2
        self.core = member % 2
        self.mate = place + 1 - 2 * (place % 2)
        self.over = 2 - self.side
        self.pair = lax.rem(place + 2, 4)
        self.sibling = member + 1 - 2 * self.core
        self.across = lax.rem(member + 2, 4)
        self.corner = self.sibling + 2 - 4 * self.chip

    def source(self, slot):
        if slot == 1:
            return self.mate
        if slot == 2:
            return self.pair
        return self.pair + 1 - 2 * (self.place % 2)


class Piece:
    def __init__(self, source, held, start, size, stride, sided, columns):
        self.source_ref = source
        self.held = held
        self.start = start
        self.size = size
        self.stride = stride
        self.sided = sided
        self.columns = columns

    def read(self, where, side):
        first = where.half * self.stride + self.start
        if self.sided == "rows":
            first = side * (2 * self.stride) + first
        rows = rows_at(first, self.size)
        if self.sided == "columns":
            columns = rows_at(side * self.columns, self.columns, LANES)
            return self.source_ref.at[rows, columns]
        return self.source_ref.at[rows]

    def target(self, where, origin, half):
        first = half * self.stride + self.start
        return self.held.at[origin, rows_at(first, self.size)]


class Stream:
    def __init__(self, where, pieces, semaphores):
        self.where = where
        self.pieces = pieces
        self.z_send, self.z_recv, self.y_send, self.y_recv = semaphores

    def z_copy(self, unit, kind):
        w, piece = self.where, self.pieces[unit]
        if kind < 2:
            side = w.side if kind == 0 else 1 - w.side
            source = piece.read(w, side)
            target = piece.target(w, w.place, w.half)
            device = w.mate if kind == 0 else w.over
            if kind == 0:
                slot = 1
            else:
                slot = 2 + w.inner.astype(jnp.int32)
        else:
            target = piece.target(w, w.source(kind), w.half)
            source = target
            device = w.mate
            slot = 5 - kind
        return pltpu.make_async_remote_copy(
            src_ref=source,
            dst_ref=target,
            send_sem=self.z_send.at[unit, kind],
            recv_sem=self.z_recv.at[unit, slot - 1],
            device_id={"fs": device},
        )

    def z_arrival(self, unit, slot):
        w = self.where
        target = self.pieces[unit].target(w, w.source(slot), w.half)
        return pltpu.make_async_remote_copy(
            src_ref=target,
            dst_ref=target,
            send_sem=self.z_send.at[unit, 0],
            recv_sem=self.z_recv.at[unit, slot - 1],
            device_id={"fs": w.mate},
        )

    def y_copy(self, unit, slot, incoming=False):
        w = self.where
        half = 1 - w.half if incoming else w.half
        target = self.pieces[unit].target(w, w.source(slot), half)
        return pltpu.make_async_remote_copy(
            src_ref=target,
            dst_ref=target,
            send_sem=self.y_send.at[unit, slot - 1],
            recv_sem=self.y_recv.at[unit, slot - 1],
            device_id={"grp": 1 - w.half},
        )

    def start(self, unit):
        self.z_copy(unit, 0).start()
        self.z_copy(unit, 1).start()

    def serve(self, unit, slot):
        self.z_arrival(unit, slot).wait_recv()
        if slot > 1:

            @pl.when(self.where.inner)
            def _():
                self.z_copy(unit, slot).start()

        self.y_copy(unit, slot).start()

    def serve_unit(self, unit):
        for slot in (1, 3, 2):
            self.serve(unit, slot)

    def arrive(self, unit):
        for slot in (1, 3, 2):
            self.y_copy(unit, slot, incoming=True).wait_recv()

    def drain(self, unit):
        self.z_copy(unit, 0).wait_send()
        self.z_copy(unit, 1).wait_send()
        for slot in (1, 2, 3):
            if slot > 1:

                @pl.when(self.where.inner)
                def _():
                    self.z_copy(unit, slot).wait_send()

            self.y_copy(unit, slot).wait_send()


class RowGather:
    def __init__(self, where, held, rows, group_rows, semaphores):
        self.where = where
        self.held = held
        self.rows = rows
        self.group_rows = group_rows
        self.send, self.recv = semaphores

    def view(self, level, member):
        first = level * self.group_rows + member * self.rows
        return self.held.at[rows_at(first, self.rows)]

    def copy(self, level, kind):
        w = self.where
        view = self.view(level, w.across if kind == 2 else w.member)
        return pltpu.make_async_remote_copy(
            src_ref=view,
            dst_ref=view,
            send_sem=self.send.at[level, kind],
            recv_sem=self.recv.at[level, kind],
            device_id={"tp": w.across if kind == 1 else w.sibling},
        )

    def arrival(self, level, kind):
        w = self.where
        member = (w.sibling, w.across, w.corner)[kind]
        view = self.view(level, member)
        return pltpu.make_async_remote_copy(
            src_ref=view,
            dst_ref=view,
            send_sem=self.send.at[level, kind],
            recv_sem=self.recv.at[level, kind],
            device_id={"tp": w.across if kind == 1 else w.sibling},
        )

    def start(self, level):
        self.copy(level, 1).start()
        self.copy(level, 0).start()

    def relay(self, level):
        self.arrival(level, 1).wait_recv()
        self.copy(level, 2).start()

    def finish(self, level):
        self.arrival(level, 0).wait_recv()
        self.arrival(level, 2).wait_recv()

    def drain(self, level):
        for kind in range(3):
            self.copy(level, kind).wait_send()

    def pair_copy(self, incoming=False):
        w = self.where
        mine = self.view(0, w.member)
        other = self.view(1, w.member)
        return pltpu.make_async_remote_copy(
            src_ref=other if incoming else mine,
            dst_ref=other,
            send_sem=self.send.at[1, 3],
            recv_sem=self.recv.at[1, 3],
            device_id={"fs": w.pair},
        )


class RowScatter:
    def __init__(self, where, levels, rows, width, part, sends, recvs, semaphores, result):
        self.where = where
        self.levels = levels
        self.rows = rows
        self.width = width
        self.part = part
        self.sends = sends
        self.recvs = recvs
        self.send_sem, self.recv_sem = semaphores
        self.result = result

    def copy(self, block, stage):
        w = self.where
        device = ({"tp": w.sibling}, {"tp": w.across}, {"fs": w.pair})[stage]
        return pltpu.make_async_remote_copy(
            src_ref=self.sends[stage].at[block],
            dst_ref=self.recvs[stage].at[block],
            send_sem=self.send_sem.at[stage, block],
            recv_sem=self.recv_sem.at[stage, block],
            device_id=device,
        )

    def begin(self, block, value):
        w = self.where
        shape = (self.levels, 2, 2, self.rows, self.width)
        self.part[block] = value.reshape(shape)
        self.sends[0][block] = self.part[block, :, :, 1 - w.core].astype(BF16)
        self.copy(block, 0).start()

    def second(self, block):
        w = self.where
        self.copy(block, 0).wait_recv()
        away = self.part[block, :, 1 - w.chip, w.core]
        away = away + self.recvs[0][block, :, 1 - w.chip].astype(F32)
        self.sends[1][block] = away.astype(BF16)
        self.copy(block, 1).start()
        kept = self.part[block, :, w.chip, w.core]
        kept = kept + self.recvs[0][block, :, w.chip].astype(F32)
        self.part[block, :, 0, 0] = kept

    def third(self, block):
        self.copy(block, 1).wait_recv()
        if self.levels > 1:
            away = self.part[block, 1, 0, 0] + self.recvs[1][block, 1].astype(F32)
            self.sends[2][block] = away.astype(BF16)
            self.copy(block, 2).start()
            kept = self.part[block, 0, 0, 0] + self.recvs[1][block, 0].astype(F32)
            self.part[block, 0, 0, 0] = kept
        else:
            self.store(block, self.part[block, 0, 0, 0] + self.recvs[1][block, 0].astype(F32))

    def fourth(self, block):
        self.copy(block, 2).wait_recv()
        self.store(block, self.part[block, 0, 0, 0] + self.recvs[2][block].astype(F32))

    def store(self, block, value):
        self.result[:, rows_at(block * self.width, self.width, LANES)] = value

    def drain(self, block):
        for stage in range(1 + self.levels):
            self.copy(block, stage).wait_send()


def layer_kernel(sizes, *refs):
    (
        tokens,
        mix_gain,
        val_weight,
        gate_weight,
        conv_taps,
        chan_gain,
        out_weight,
        mix_post_gain,
        ffn_gain,
        up_gate_weight,
        up_val_weight,
        ffn_taps,
        down_weight,
        ffn_post_gain,
        layer_out,
        val_all,
        gate_all,
        out_all,
        up_gate_all,
        up_val_all,
        down_all,
        mix_rows,
        ffn_rows,
        glu_padded,
        conv_out,
        stats,
        activated,
        up_padded,
        hidden,
        residual_ref,
        result,
        mix_part,
        ffn_part,
        mix_send0,
        mix_send1,
        mix_recv0,
        mix_recv1,
        ffn_send0,
        ffn_send1,
        ffn_send2,
        ffn_recv0,
        ffn_recv1,
        ffn_recv2,
        own_sem,
        z_send,
        z_recv,
        y_send,
        y_recv,
        mix_row_send,
        mix_row_recv,
        ffn_row_send,
        ffn_row_recv,
        stat_send,
        stat_recv,
        mix_sum_send,
        mix_sum_recv,
        ffn_sum_send,
        ffn_sum_recv,
    ) = refs
    w = Where()
    rows, group_rows, segments = sizes["rows"], sizes["group_rows"], sizes["segments"]
    depth, local_ch, half_ff = sizes["depth"], sizes["local_ch"], sizes["half_ff"]
    width = out_all.shape[2]
    mix_tiles, ffn_tiles = local_ch // LANES, half_ff // LANES
    member = w.member

    barrier = pltpu.get_barrier_semaphore()
    friends = [
        {"tp": w.sibling},
        {"tp": w.across},
        {"tp": w.corner},
        {"grp": 1 - w.half},
        {"fs": w.mate},
        {"fs": w.pair},
    ]
    for friend in friends:
        pl.semaphore_signal(barrier, inc=1, device_id=friend)

    @pl.when(w.inner)
    def _():
        pl.semaphore_signal(barrier, inc=1, device_id={"fs": 3 - w.place})

    pieces = []

    def cut(source, held, sided, chunks):
        total = held.shape[1] // 2
        size = total // chunks
        return [
            Piece(source, held, index * size, size, total, sided, held.shape[2])
            for index in range(chunks)
        ]

    val_pieces = cut(val_weight, val_all, None, 2)
    gate_pieces = cut(gate_weight, gate_all, None, 2)
    out_pieces = cut(out_weight, out_all, None, 2)
    up_gate_pieces = cut(up_gate_weight, up_gate_all, "columns", 2)
    up_val_pieces = cut(up_val_weight, up_val_all, "columns", 2)
    down_pieces = cut(down_weight, down_all, "rows", sizes["down_chunks"])
    first = [val_pieces[0], gate_pieces[0], val_pieces[1], gate_pieces[1]]
    later = [up_gate_pieces[0], up_val_pieces[0], up_gate_pieces[1], up_val_pieces[1]]
    pieces = first + out_pieces + later + down_pieces
    proj = list(range(0, 4))
    outs = list(range(4, 6))
    ups = list(range(6, 10))
    downs = list(range(10, 10 + len(down_pieces)))
    stream = Stream(w, pieces, (z_send, z_recv, y_send, y_recv))

    def own_copy(index, source, held, sided):
        if sided == "columns":
            view = source.at[:, rows_at(w.side * held.shape[2], held.shape[2], LANES)]
        elif sided == "rows":
            view = source.at[rows_at(w.side * held.shape[1], held.shape[1])]
        else:
            view = source
        return pltpu.make_async_copy(view, held.at[w.place], own_sem.at[index])

    own_copies = [
        own_copy(0, val_weight, val_all, None),
        own_copy(1, gate_weight, gate_all, None),
        own_copy(2, out_weight, out_all, None),
        own_copy(3, up_gate_weight, up_gate_all, "columns"),
        own_copy(4, up_val_weight, up_val_all, "columns"),
        own_copy(5, down_weight, down_all, "rows"),
    ]
    for copy in own_copies:
        copy.start()

    glu_padded[:, 0:32, :] = jnp.zeros((glu_padded.shape[0], 32, LANES), F32)
    up_padded[:, :, 0:8, :] = jnp.zeros((2, up_padded.shape[1], 8, LANES), F32)
    own_rows = rows_at(member * rows, rows)
    mix_rows[own_rows] = rms_scale(tokens[...].astype(F32), mix_gain[...]).astype(BF16)

    pl.semaphore_wait(barrier, len(friends) + w.inner.astype(jnp.int32))

    for unit in proj + outs:
        stream.start(unit)
    mix_gather = RowGather(w, mix_rows, rows, group_rows, (mix_row_send, mix_row_recv))
    mix_gather.start(0)
    stream.serve_unit(0)
    stream.serve_unit(1)
    mix_gather.relay(0)
    stream.serve_unit(2)
    stream.serve_unit(3)
    stream.serve_unit(4)
    for unit in ups[:2]:
        stream.start(unit)
    for unit in proj:
        stream.arrive(unit)
    own_copies[0].wait()
    own_copies[1].wait()
    mix_gather.finish(0)

    left = mix_rows[...]
    values = product(left, val_all[...].reshape(depth, local_ch))
    gate_sums = product(left, gate_all[...].reshape(depth, local_ch))
    glu = (values * jax.nn.sigmoid(gate_sums)).astype(BF16).astype(F32)
    for tile in range(mix_tiles):
        block = glu[:, tile * LANES : (tile + 1) * LANES].reshape(segments, LEN, LANES)
        glu_padded[tile * segments : (tile + 1) * segments, 32:, :] = block
    stream.serve_unit(5)
    for unit in ups[2:]:
        stream.start(unit)

    taps_count = conv_taps.shape[0]
    for tile in range(mix_tiles):
        lanes = rows_at(member * local_ch + tile * LANES, LANES, LANES)
        taps = conv_taps[:, lanes].astype(F32)

        @pl.loop(0, segments)
        def _(segment):
            total = jnp.zeros((LEN, LANES), F32)
            for k in range(taps_count):
                shifted = glu_padded[tile * segments + segment, pl.ds(33 - taps_count + k, LEN), :]
                total = total + shifted * taps[k : k + 1]
            conv_out[tile, rows_at(segment * LEN, LEN)] = total

    sums = conv_out[0]
    squares = conv_out[0] * conv_out[0]
    for tile in range(1, mix_tiles):
        sums = sums + conv_out[tile]
        squares = squares + conv_out[tile] * conv_out[tile]
    exact = lax.Precision.HIGHEST
    ones = jnp.ones((8, LANES), F32)
    contract_lanes = (((1,), (1,)), ((), ()))
    sums = lax.dot_general(ones, sums, contract_lanes, precision=exact, preferred_element_type=F32)
    squares = lax.dot_general(
        ones, squares, contract_lanes, precision=exact, preferred_element_type=F32
    )
    upper = lax.broadcasted_iota(jnp.int32, (8, group_rows), 0) < 4
    stats[0, :, :] = jnp.zeros(stats.shape[1:], F32)
    stats[0, :, 0:group_rows] = jnp.where(upper, sums, squares)

    def stat_copy(kind):
        device = (w.sibling, w.across, w.corner)[kind]
        return pltpu.make_async_remote_copy(
            src_ref=stats.at[0],
            dst_ref=stats.at[1 + kind],
            send_sem=stat_send.at[kind],
            recv_sem=stat_recv.at[kind],
            device_id={"tp": device},
        )

    for kind in (2, 1, 0):
        stat_copy(kind).start()
    stream.serve_unit(6)
    for unit in outs:
        stream.arrive(unit)
    own_copies[2].wait()
    for kind in range(3):
        stat_copy(kind).wait_recv()
    total = stats[0] + stats[1] + stats[2] + stats[3]
    flipped = jnp.transpose(total)[:group_rows] / chan_gain.shape[1]
    chan_mean = flipped[:, 0:1]
    chan_var = flipped[:, 4:5] - chan_mean * chan_mean
    inverse = lax.rsqrt(chan_var + chan_epsilon)
    for tile in range(mix_tiles):
        lanes = rows_at(member * local_ch + tile * LANES, LANES, LANES)
        scaled = (conv_out[tile] - chan_mean) * inverse * chan_gain[:, lanes].astype(F32)
        activated[:, tile * LANES : (tile + 1) * LANES] = jax.nn.silu(scaled).astype(BF16)

    mix_sum = RowScatter(
        w,
        1,
        rows,
        width,
        mix_part,
        (mix_send0, mix_send1),
        (mix_recv0, mix_recv1),
        (mix_sum_send, mix_sum_recv),
        result,
    )
    places = [w.place, w.mate, w.source(3), w.source(2)]
    for index in range(4 + 2):
        if index < 4:
            block = places[index]
            mix_sum.begin(block, product(activated[...], out_all[block]))
        if 1 <= index < 5:
            mix_sum.second(places[index - 1])
        if 2 <= index:
            mix_sum.third(places[index - 2])

    residual = tokens[...].astype(F32) + rms_scale(result[...], mix_post_gain[...])
    residual = residual.astype(BF16)
    residual_ref[...] = residual
    ffn_rows[own_rows] = rms_scale(residual.astype(F32), ffn_gain[...]).astype(BF16)
    ffn_gather = RowGather(w, ffn_rows, rows, group_rows, (ffn_row_send, ffn_row_recv))
    ffn_gather.start(0)
    ffn_gather.pair_copy().start()
    for unit in downs[:2]:
        stream.start(unit)
    stream.serve_unit(7)
    ffn_gather.relay(0)
    stream.serve_unit(8)
    ffn_gather.pair_copy(incoming=True).wait_recv()
    ffn_gather.start(1)
    stream.serve_unit(9)
    for unit in downs[2:]:
        stream.start(unit)
    ffn_gather.relay(1)
    stream.serve_unit(downs[0])
    for unit in ups:
        stream.arrive(unit)
    own_copies[3].wait()
    own_copies[4].wait()

    def feed(level):
        ffn_gather.finish(level)
        left = ffn_rows[level * group_rows : (level + 1) * group_rows]
        for half, weight in enumerate((up_gate_all, up_val_all)):
            up = product(left, weight[...].reshape(depth, half_ff)).astype(BF16).astype(F32)
            for tile in range(ffn_tiles):
                block = up[:, tile * LANES : (tile + 1) * LANES].reshape(segments, LEN, LANES)
                up_padded[half, tile * segments : (tile + 1) * segments, 8:, :] = block
        for tile in range(ffn_tiles):
            first_lane = (2 * member + w.side) * half_ff + tile * LANES
            lanes = rows_at(first_lane, LANES, LANES)
            taps = [ffn_taps[half, :, lanes].astype(F32) for half in range(2)]

            @pl.loop(0, segments)
            def _(segment):
                convs = []
                for half in range(2):
                    conv = jnp.zeros((LEN, LANES), F32)
                    count = ffn_taps.shape[1]
                    for k in range(count):
                        shifted = up_padded[
                            half, tile * segments + segment, pl.ds(9 - count + k, LEN), :
                        ]
                        conv = conv + shifted * taps[half][k : k + 1]
                    convs.append(conv)
                value = jax.nn.gelu(convs[0], approximate=True) * convs[1]
                at = rows_at(level * group_rows + segment * LEN, LEN)
                hidden[at, tile * LANES : (tile + 1) * LANES] = value.astype(BF16)

    feed(0)
    stream.serve_unit(downs[1])
    feed(1)
    for unit in downs[2:]:
        stream.serve_unit(unit)
    ffn_sum = RowScatter(
        w,
        2,
        rows,
        width,
        ffn_part,
        (ffn_send0, ffn_send1, ffn_send2),
        (ffn_recv0, ffn_recv1, ffn_recv2),
        (ffn_sum_send, ffn_sum_recv),
        result,
    )
    own_copies[5].wait()
    slots = [None, 1, 3, 2]
    for index in range(4 + 2):
        if index < 4:
            block = places[index]
            if index > 0:
                for unit in downs:
                    stream.y_copy(unit, slots[index], incoming=True).wait_recv()
            ffn_sum.begin(block, product(hidden[...], down_all[block]))
        if 1 <= index < 5:
            ffn_sum.second(places[index - 1])
        if 2 <= index:
            ffn_sum.third(places[index - 2])
    for index in (3, 2, 1, 0):
        ffn_sum.fourth(places[3 - index])
    final = residual_ref[...].astype(F32) + rms_scale(result[...], ffn_post_gain[...])
    layer_out[...] = final.astype(BF16)

    for unit in range(len(pieces)):
        stream.drain(unit)
    mix_gather.drain(0)
    ffn_gather.drain(0)
    ffn_gather.drain(1)
    ffn_gather.pair_copy().wait_send()
    for kind in range(3):
        stat_copy(kind).wait_send()
    for index in range(4):
        mix_sum.drain(places[index])
        ffn_sum.drain(places[index])


def kernel_sizes(tokens, val_weight, out_weight, up_gate_weight, down_weight):
    rows = tokens.shape[0]
    return {
        "rows": rows,
        "group_rows": 4 * rows,
        "segments": 4 * rows // LEN,
        "depth": 4 * val_weight.shape[0],
        "local_ch": val_weight.shape[1],
        "half_ff": up_gate_weight.shape[1] // 2,
        "down_chunks": 4,
    }


def run_kernel(*args):
    (
        tokens,
        mix_gain,
        val_weight,
        gate_weight,
        conv_taps,
        chan_gain,
        out_weight,
        mix_post_gain,
        ffn_gain,
        up_gate_weight,
        up_val_weight,
        ffn_taps,
        down_weight,
        ffn_post_gain,
    ) = args
    sizes = kernel_sizes(tokens, val_weight, out_weight, up_gate_weight, down_weight)
    rows, group_rows, segments = sizes["rows"], sizes["group_rows"], sizes["segments"]
    local_ch, half_ff = sizes["local_ch"], sizes["half_ff"]
    width = out_weight.shape[1]
    model = tokens.shape[1]
    mix_tiles, ffn_tiles = local_ch // LANES, half_ff // LANES
    padded_rows = -(-group_rows // LANES) * LANES
    units = 10 + sizes["down_chunks"]
    dma = pltpu.SemaphoreType.DMA
    vmem, anywhere = pl.BlockSpec(memory_space=pltpu.VMEM), pl.BlockSpec(memory_space=pl.ANY)
    shaped = [
        tokens,
        mix_gain[None],
        val_weight,
        gate_weight,
        conv_taps,
        chan_gain[None],
        out_weight,
        mix_post_gain[None],
        ffn_gain[None],
        up_gate_weight,
        up_val_weight,
        ffn_taps,
        down_weight,
        ffn_post_gain[None],
    ]
    weights = (2, 3, 6, 9, 10, 12)
    scratch = [
        pltpu.VMEM((4, val_weight.shape[0], local_ch), BF16),
        pltpu.VMEM((4, gate_weight.shape[0], local_ch), BF16),
        pltpu.VMEM((4, local_ch, width), BF16),
        pltpu.VMEM((4, up_gate_weight.shape[0], half_ff), BF16),
        pltpu.VMEM((4, up_val_weight.shape[0], half_ff), BF16),
        pltpu.VMEM((4, half_ff, width), BF16),
        pltpu.VMEM((group_rows, model), BF16),
        pltpu.VMEM((2 * group_rows, model), BF16),
        pltpu.VMEM((mix_tiles * segments, 32 + LEN, LANES), F32),
        pltpu.VMEM((mix_tiles, group_rows, LANES), F32),
        pltpu.VMEM((4, 8, padded_rows), F32),
        pltpu.VMEM((group_rows, local_ch), BF16),
        pltpu.VMEM((2, ffn_tiles * segments, 8 + LEN, LANES), F32),
        pltpu.VMEM((2 * group_rows, half_ff), BF16),
        pltpu.VMEM((rows, model), BF16),
        pltpu.VMEM((rows, model), F32),
        pltpu.VMEM((4, 1, 2, 2, rows, width), F32),
        pltpu.VMEM((4, 2, 2, 2, rows, width), F32),
        pltpu.VMEM((4, 1, 2, rows, width), BF16),
        pltpu.VMEM((4, 1, rows, width), BF16),
        pltpu.VMEM((4, 1, 2, rows, width), BF16),
        pltpu.VMEM((4, 1, rows, width), BF16),
        pltpu.VMEM((4, 2, 2, rows, width), BF16),
        pltpu.VMEM((4, 2, rows, width), BF16),
        pltpu.VMEM((4, rows, width), BF16),
        pltpu.VMEM((4, 2, 2, rows, width), BF16),
        pltpu.VMEM((4, 2, rows, width), BF16),
        pltpu.VMEM((4, rows, width), BF16),
        dma((6,)),
        dma((units, 4)),
        dma((units, 3)),
        dma((units, 3)),
        dma((units, 3)),
        dma((1, 3)),
        dma((1, 3)),
        dma((2, 4)),
        dma((2, 4)),
        dma((3,)),
        dma((3,)),
        dma((2, 4)),
        dma((2, 4)),
        dma((3, 4)),
        dma((3, 4)),
    ]
    return pl.pallas_call(
        functools.partial(layer_kernel, sizes),
        out_shape=jax.ShapeDtypeStruct(tokens.shape, BF16),
        in_specs=[anywhere if index in weights else vmem for index in range(len(shaped))],
        out_specs=vmem,
        scratch_shapes=scratch,
        compiler_params=pltpu.CompilerParams(
            collective_id=0, has_side_effects=True, vmem_limit_bytes=56_000_000
        ),
    )(*shaped)


def fits(mesh, args):
    tokens, val_weight, out_weight = args[0], args[2], args[6]
    up_gate_weight, down_weight = args[9], args[12]
    if (mesh.shape["grp"], mesh.shape["fs"], mesh.shape["tp"]) != (2, 4, 4):
        return False
    rows = tokens.shape[0] // 32
    local_ch, local_ff = val_weight.shape[1] // 4, up_gate_weight.shape[1] // 4
    local_model = tokens.shape[1] // 4
    return (
        rows % 16 == 0
        and 4 * rows % LEN == 0
        and local_ch % LANES == 0
        and local_ff % (2 * LANES) == 0
        and local_model % LANES == 0
        and args[4].shape[0] <= 32
        and args[11].shape[1] <= 8
    )


def solution(mesh):
    specs = (
        P(("grp", "fs", "tp"), None),
        P(),
        P("fs", "tp"),
        P("fs", "tp"),
        P(),
        P(),
        P("tp", "fs"),
        P(),
        P(),
        P("fs", "tp"),
        P("fs", "tp"),
        P(),
        P("tp", "fs"),
        P(),
    )

    def whole(*args):
        body = run_kernel if fits(mesh, args) else plain
        step = jax.shard_map(
            body,
            mesh=mesh,
            in_specs=specs,
            out_specs=P(("grp", "fs", "tp"), None),
            check_vma=False,
        )
        return step(*args)

    return whole
```

profile of v0, /device:TPU:8, one launch (start us, length us, event | category | flops | bytes accessed | tf_op | source)
XLA Modules:
  0.0 150.6 jit_solution(13104498466324380214)
XLA Ops:
  0.0 0.7 broadcast_in_dim.16.refs_5_
  0.7 0.7 broadcast_in_dim.15.refs_1_
  1.4 0.7 broadcast_in_dim.17.refs_7_
  2.1 0.7 broadcast_in_dim.18.refs_8_
  2.8 0.7 broadcast_in_dim.19.refs_13_
  3.5 0.9 copy.15.refs_11_
  4.3 0.0 copy-start
  4.3 0.9 copy-done
  5.3 0.0 copy-start.1
  5.3 0.8 copy-done.1
  6.1 142.8 %shard_map.136 = bf16[80,2048]{1,0:T(8,128)(2,1)} custom-call(bf16[80,2048]{1,0:T(8,128)(2,1)} %refs_0_.1, bf16[1,2048]{1,0:T(2,128)(2,1)S(1)} %broadcast_in_dim.15.refs_1_, bf16[512,256]{1,0:T(8,128)(2,1)S(1)} %copy-done, bf16[512,256]{1,0:T(8,128)(2,1)} %refs_3_.1, bf16[31,1024]{1,0:T(8,128)(2,1)S(1)} %copy-done.1, ...), custom_call_target="tpu_custom_call" | custom-call | tf_op jit(solution)/shard_map/pallas_call | solution.py:817
  148.9 1.7 %copy.17 = bf16[80,2048]{1,0:T(8,128)(2,1)} copy(bf16[80,2048]{1,0:T(8,128)(2,1)} %shard_map.136) | data formatting | bytes 655360
Async XLA Ops:
  4.3 1.0 copy-start
  5.3 0.8 copy-start.1
where the time goes:
time: 151 us
  Pallas kernels  143 us (95%)
  local copies, waits for them, and re-layouts  7.82 us (5%)
    pallas_call x1, Pallas kernels, run_kernel(): pl.pallas_call(functools.partial(layer_kernel, sizes), out_shape=jax.Shap...  143 us
    unnamed x6, local copies, waits for them, and re-layouts  4.36 us

commit v1 on v0

--- a/solution.py
+++ b/solution.py
@@ -210,19 +210,39 @@
         self.z_copy(unit, 0).start()
         self.z_copy(unit, 1).start()
 
-    def serve(self, unit, slot):
+    def serve(self, unit, slot, relay):
         self.z_arrival(unit, slot).wait_recv()
-        if slot > 1:
-
-            @pl.when(self.where.inner)
-            def _():
-                self.z_copy(unit, slot).start()
-
+        if relay:
+            self.z_copy(unit, slot).start()
         self.y_copy(unit, slot).start()
 
-    def serve_unit(self, unit):
-        for slot in (1, 3, 2):
-            self.serve(unit, slot)
+    def events(self, order, ahead, lag):
+        count = len(order)
+        inner, outer = [], []
+        for index in range(count + lag):
+            first = [order[index + ahead]] if index + ahead < count else []
+            for slot in (2, 3, 1):
+                if index < count:
+                    begin = first if slot == 2 else []
+                    inner.append((begin, order[index], slot, slot > 1))
+            if index < count:
+                outer.append((first, order[index], 1, False))
+            if index >= lag:
+                outer.append(([], order[index - lag], 3, False))
+                outer.append(([], order[index - lag], 2, False))
+        self.waiting = list(zip(inner, outer))
+
+    def pump(self, count):
+        for _ in range(min(count, len(self.waiting))):
+            pair = self.waiting.pop(0)
+            for role, (begin, unit, slot, relay) in enumerate(pair):
+                chosen = jnp.logical_not(self.where.inner) if role else self.where.inner
+
+                @pl.when(chosen)
+                def _():
+                    for other in begin:
+                        self.start(other)
+                    self.serve(unit, slot, relay)
 
     def arrive(self, unit):
         for slot in (1, 3, 2):
@@ -386,6 +406,14 @@
         down_weight,
         ffn_post_gain,
         layer_out,
+        tokens_in,
+        conv_taps_in,
+        ffn_taps_in,
+        mix_gain_in,
+        chan_gain_in,
+        mix_post_gain_in,
+        ffn_gain_in,
+        ffn_post_gain_in,
         val_all,
         gate_all,
         out_all,
@@ -414,6 +442,8 @@
         ffn_recv0,
         ffn_recv1,
         ffn_recv2,
+        out_staged,
+        load_sem,
         own_sem,
         z_send,
         z_recv,
@@ -495,28 +525,45 @@
         own_copy(4, up_val_weight, up_val_all, "columns"),
         own_copy(5, down_weight, down_all, "rows"),
     ]
-    for copy in own_copies:
+    small = [
+        (tokens, tokens_in),
+        (mix_gain, mix_gain_in),
+        (conv_taps, conv_taps_in),
+        (chan_gain, chan_gain_in),
+        (mix_post_gain, mix_post_gain_in),
+        (ffn_gain, ffn_gain_in),
+        (ffn_taps, ffn_taps_in),
+        (ffn_post_gain, ffn_post_gain_in),
+    ]
+    loads = [
+        pltpu.make_async_copy(source, held, load_sem.at[index])
+        for index, (source, held) in enumerate(small)
+    ]
+    for copy in loads + own_copies:
         copy.start()
 
     glu_padded[:, 0:32, :] = jnp.zeros((glu_padded.shape[0], 32, LANES), F32)
     up_padded[:, :, 0:8, :] = jnp.zeros((2, up_padded.shape[1], 8, LANES), F32)
     own_rows = rows_at(member * rows, rows)
-    mix_rows[own_rows] = rms_scale(tokens[...].astype(F32), mix_gain[...]).astype(BF16)
+
+    def gain_of(held):
+        return held[...].astype(F32).reshape(1, held.shape[0])
+
+    loads[0].wait()
+    loads[1].wait()
+    mix_rows[own_rows] = rms_scale(tokens_in[...].astype(F32), gain_of(mix_gain_in)).astype(BF16)
 
     pl.semaphore_wait(barrier, len(friends) + w.inner.astype(jnp.int32))
 
-    for unit in proj + outs:
+    ahead = 2
+    for unit in range(ahead):
         stream.start(unit)
     mix_gather = RowGather(w, mix_rows, rows, group_rows, (mix_row_send, mix_row_recv))
     mix_gather.start(0)
-    stream.serve_unit(0)
-    stream.serve_unit(1)
+    stream.events(list(range(len(pieces))), ahead, 2)
+    stream.pump(9)
     mix_gather.relay(0)
-    stream.serve_unit(2)
-    stream.serve_unit(3)
-    stream.serve_unit(4)
-    for unit in ups[:2]:
-        stream.start(unit)
+    stream.pump(8)
     for unit in proj:
         stream.arrive(unit)
     own_copies[0].wait()
@@ -530,14 +577,14 @@
     for tile in range(mix_tiles):
         block = glu[:, tile * LANES : (tile + 1) * LANES].reshape(segments, LEN, LANES)
         glu_padded[tile * segments : (tile + 1) * segments, 32:, :] = block
-    stream.serve_unit(5)
-    for unit in ups[2:]:
-        stream.start(unit)
+    stream.pump(1)
 
     taps_count = conv_taps.shape[0]
+    loads[2].wait()
+    loads[3].wait()
     for tile in range(mix_tiles):
         lanes = rows_at(member * local_ch + tile * LANES, LANES, LANES)
-        taps = conv_taps[:, lanes].astype(F32)
+        taps = conv_taps_in[:, lanes].astype(F32)
 
         @pl.loop(0, segments)
         def _(segment):
@@ -575,20 +622,21 @@
 
     for kind in (2, 1, 0):
         stat_copy(kind).start()
-    stream.serve_unit(6)
+    stream.pump(2)
     for unit in outs:
         stream.arrive(unit)
     own_copies[2].wait()
     for kind in range(3):
         stat_copy(kind).wait_recv()
     total = stats[0] + stats[1] + stats[2] + stats[3]
-    flipped = jnp.transpose(total)[:group_rows] / chan_gain.shape[1]
+    flipped = jnp.transpose(total)[:group_rows] / chan_gain.shape[0]
     chan_mean = flipped[:, 0:1]
     chan_var = flipped[:, 4:5] - chan_mean * chan_mean
     inverse = lax.rsqrt(chan_var + chan_epsilon)
+    chan_gains = chan_gain_in[rows_at(member * local_ch, local_ch, LANES)].astype(F32)
+    chan_gains = chan_gains.reshape(1, local_ch)
     for tile in range(mix_tiles):
-        lanes = rows_at(member * local_ch + tile * LANES, LANES, LANES)
-        scaled = (conv_out[tile] - chan_mean) * inverse * chan_gain[:, lanes].astype(F32)
+        scaled = (conv_out[tile] - chan_mean) * inverse * chan_gains[:, tile * LANES : (tile + 1) * LANES]
         activated[:, tile * LANES : (tile + 1) * LANES] = jax.nn.silu(scaled).astype(BF16)
 
     mix_sum = RowScatter(
@@ -611,30 +659,31 @@
             mix_sum.second(places[index - 1])
         if 2 <= index:
             mix_sum.third(places[index - 2])
-
-    residual = tokens[...].astype(F32) + rms_scale(result[...], mix_post_gain[...])
+        if index % 2 == 1:
+            stream.pump(1)
+
+    loads[4].wait()
+    loads[5].wait()
+    residual = tokens_in[...].astype(F32) + rms_scale(result[...], gain_of(mix_post_gain_in))
     residual = residual.astype(BF16)
     residual_ref[...] = residual
-    ffn_rows[own_rows] = rms_scale(residual.astype(F32), ffn_gain[...]).astype(BF16)
+    ffn_rows[own_rows] = rms_scale(residual.astype(F32), gain_of(ffn_gain_in)).astype(BF16)
     ffn_gather = RowGather(w, ffn_rows, rows, group_rows, (ffn_row_send, ffn_row_recv))
     ffn_gather.start(0)
     ffn_gather.pair_copy().start()
-    for unit in downs[:2]:
-        stream.start(unit)
-    stream.serve_unit(7)
+    stream.pump(1)
     ffn_gather.relay(0)
-    stream.serve_unit(8)
+    stream.pump(2)
     ffn_gather.pair_copy(incoming=True).wait_recv()
     ffn_gather.start(1)
-    stream.serve_unit(9)
-    for unit in downs[2:]:
-        stream.start(unit)
+    stream.pump(2)
     ffn_gather.relay(1)
-    stream.serve_unit(downs[0])
+    stream.pump(6)
     for unit in ups:
         stream.arrive(unit)
     own_copies[3].wait()
     own_copies[4].wait()
+    loads[6].wait()
 
     def feed(level):
         ffn_gather.finish(level)
@@ -644,17 +693,18 @@
             for tile in range(ffn_tiles):
                 block = up[:, tile * LANES : (tile + 1) * LANES].reshape(segments, LEN, LANES)
                 up_padded[half, tile * segments : (tile + 1) * segments, 8:, :] = block
+            stream.pump(1)
         for tile in range(ffn_tiles):
             first_lane = (2 * member + w.side) * half_ff + tile * LANES
             lanes = rows_at(first_lane, LANES, LANES)
-            taps = [ffn_taps[half, :, lanes].astype(F32) for half in range(2)]
+            taps = [ffn_taps_in[:, half, lanes].astype(F32) for half in range(2)]
 
             @pl.loop(0, segments)
             def _(segment):
                 convs = []
                 for half in range(2):
                     conv = jnp.zeros((LEN, LANES), F32)
-                    count = ffn_taps.shape[1]
+                    count = ffn_taps.shape[0]
                     for k in range(count):
                         shifted = up_padded[
                             half, tile * segments + segment, pl.ds(9 - count + k, LEN), :
@@ -666,10 +716,8 @@
                 hidden[at, tile * LANES : (tile + 1) * LANES] = value.astype(BF16)
 
     feed(0)
-    stream.serve_unit(downs[1])
+    stream.pump(1)
     feed(1)
-    for unit in downs[2:]:
-        stream.serve_unit(unit)
     ffn_sum = RowScatter(
         w,
         2,
@@ -683,9 +731,12 @@
     )
     own_copies[5].wait()
     slots = [None, 1, 3, 2]
+    stream.pump(1)
     for index in range(4 + 2):
         if index < 4:
             block = places[index]
+            if index == 1:
+                stream.pump(len(stream.waiting))
             if index > 0:
                 for unit in downs:
                     stream.y_copy(unit, slots[index], incoming=True).wait_recv()
@@ -696,8 +747,11 @@
             ffn_sum.third(places[index - 2])
     for index in (3, 2, 1, 0):
         ffn_sum.fourth(places[3 - index])
-    final = residual_ref[...].astype(F32) + rms_scale(result[...], ffn_post_gain[...])
-    layer_out[...] = final.astype(BF16)
+    loads[7].wait()
+    final = residual_ref[...].astype(F32) + rms_scale(result[...], gain_of(ffn_post_gain_in))
+    out_staged[...] = final.astype(BF16)
+    leave = pltpu.make_async_copy(out_staged, layer_out, load_sem.at[len(small)])
+    leave.start()
 
     for unit in range(len(pieces)):
         stream.drain(unit)
@@ -710,6 +764,7 @@
     for index in range(4):
         mix_sum.drain(places[index])
         ffn_sum.drain(places[index])
+    leave.wait()
 
 
 def kernel_sizes(tokens, val_weight, out_weight, up_gate_weight, down_weight):
@@ -751,25 +806,31 @@
     padded_rows = -(-group_rows // LANES) * LANES
     units = 10 + sizes["down_chunks"]
     dma = pltpu.SemaphoreType.DMA
-    vmem, anywhere = pl.BlockSpec(memory_space=pltpu.VMEM), pl.BlockSpec(memory_space=pl.ANY)
     shaped = [
         tokens,
-        mix_gain[None],
+        mix_gain,
         val_weight,
         gate_weight,
         conv_taps,
-        chan_gain[None],
+        chan_gain,
         out_weight,
-        mix_post_gain[None],
-        ffn_gain[None],
+        mix_post_gain,
+        ffn_gain,
         up_gate_weight,
         up_val_weight,
-        ffn_taps,
+        jnp.transpose(ffn_taps, (1, 0, 2)),
         down_weight,
-        ffn_post_gain[None],
+        ffn_post_gain,
     ]
-    weights = (2, 3, 6, 9, 10, 12)
     scratch = [
+        pltpu.VMEM(tokens.shape, BF16),
+        pltpu.VMEM(conv_taps.shape, BF16),
+        pltpu.VMEM(shaped[11].shape, BF16),
+        pltpu.VMEM(mix_gain.shape, BF16),
+        pltpu.VMEM(chan_gain.shape, BF16),
+        pltpu.VMEM(mix_post_gain.shape, BF16),
+        pltpu.VMEM(ffn_gain.shape, BF16),
+        pltpu.VMEM(ffn_post_gain.shape, BF16),
         pltpu.VMEM((4, val_weight.shape[0], local_ch), BF16),
         pltpu.VMEM((4, gate_weight.shape[0], local_ch), BF16),
         pltpu.VMEM((4, local_ch, width), BF16),
@@ -798,6 +859,8 @@
         pltpu.VMEM((4, 2, 2, rows, width), BF16),
         pltpu.VMEM((4, 2, rows, width), BF16),
         pltpu.VMEM((4, rows, width), BF16),
+        pltpu.VMEM(tokens.shape, BF16),
+        dma((9,)),
         dma((6,)),
         dma((units, 4)),
         dma((units, 3)),
@@ -817,11 +880,11 @@
     return pl.pallas_call(
         functools.partial(layer_kernel, sizes),
         out_shape=jax.ShapeDtypeStruct(tokens.shape, BF16),
-        in_specs=[anywhere if index in weights else vmem for index in range(len(shaped))],
-        out_specs=vmem,
+        in_specs=[pl.BlockSpec(memory_space=pltpu.HBM)] * len(shaped),
+        out_specs=pl.BlockSpec(memory_space=pl.ANY),
         scratch_shapes=scratch,
         compiler_params=pltpu.CompilerParams(
-            collective_id=0, has_side_effects=True, vmem_limit_bytes=56_000_000
+            collective_id=0, has_side_effects=True, vmem_limit_bytes=67_043_328
         ),
     )(*shaped)
 

time: 151 us -> 131 us (0.87)
  Pallas kernels: 143 us -> 129 us
  local copies, waits for them, and re-layouts: 7.82 us -> 1.72 us
    pallas_call x1, Pallas kernels: 143 us -> 129 us  [run_kernel(): pl.pallas_call(functools.partial(layer_kernel, sizes), out_shape=jax.Shap...]
    broadcast_in_dim x5 -> x0, local copies, waits for them, and re-layouts: 3.46 us -> none  [the longest x1 0.69 us: run_kernel(): mix_gain[None]]
    unnamed x6 -> x1, local copies, waits for them, and re-layouts: 4.36 us -> 1.72 us
where the time goes in v1:
time: 131 us
  Pallas kernels  129 us (98%)
  local copies, waits for them, and re-layouts  1.72 us (1%)
    pallas_call x1, Pallas kernels, run_kernel(): pl.pallas_call(functools.partial(layer_kernel, sizes), out_shape=jax.Shap...  129 us

profile of v1, /device:TPU:8, one launch (start us, length us, event | category | flops | bytes accessed | tf_op | source)
XLA Modules:
  0.0 131.1 jit_solution(6997413483311319248)
XLA Ops:
  0.0 129.4 %shard_map.136 = bf16[80,2048]{1,0:T(8,128)(2,1)} custom-call(bf16[80,2048]{1,0:T(8,128)(2,1)} %refs_0_.1, bf16[2048]{0:T(1024)(128)(2,1)} %refs_1_.1, bf16[512,256]{1,0:T(8,128)(2,1)} %refs_2_.1, bf16[512,256]{1,0:T(8,128)(2,1)} %refs_3_.1, bf16[31,1024]{1,0:T(8,128)(2,1)} %refs_4_.1, bf16[1024]{0:T(1024)(128)(2,1)} %refs_5_.1, bf16[256,512]{1,0:T(8,128)(2,1)} %refs_6_.1, ...), custom_call_target="tpu_custom_call" | custom-call | tf_op jit(solution)/shard_map/pallas_call | solution.py:880
  129.4 1.7 %copy.16 = bf16[80,2048]{1,0:T(8,128)(2,1)} copy(bf16[80,2048]{1,0:T(8,128)(2,1)} %shard_map.136) | data formatting | bytes 655360

commit v2 on v1

--- a/solution.py
+++ b/solution.py
@@ -9,6 +9,9 @@
 
 LEN = 64
 LANES = 128
+SUMS = 1
+UP_CUTS = 4
+AHEAD = 2
 F32 = jnp.float32
 BF16 = jnp.bfloat16
 
@@ -129,7 +132,7 @@
 
 
 class Piece:
-    def __init__(self, source, held, start, size, stride, sided, columns):
+    def __init__(self, source, held, start, size, stride, sided, columns, lanes=None):
         self.source_ref = source
         self.held = held
         self.start = start
@@ -137,6 +140,7 @@
         self.stride = stride
         self.sided = sided
         self.columns = columns
+        self.lanes = lanes
 
     def read(self, where, side):
         first = where.half * self.stride + self.start
@@ -146,11 +150,16 @@
         if self.sided == "columns":
             columns = rows_at(side * self.columns, self.columns, LANES)
             return self.source_ref.at[rows, columns]
+        if self.lanes is not None:
+            return self.source_ref.at[rows, self.lanes]
         return self.source_ref.at[rows]
 
     def target(self, where, origin, half):
         first = half * self.stride + self.start
-        return self.held.at[origin, rows_at(first, self.size)]
+        rows = rows_at(first, self.size)
+        if self.lanes is not None:
+            return self.held.at[origin, rows, self.lanes]
+        return self.held.at[origin, rows]
 
 
 class Stream:
@@ -216,21 +225,33 @@
             self.z_copy(unit, slot).start()
         self.y_copy(unit, slot).start()
 
-    def events(self, order, ahead, lag):
-        count = len(order)
+    def events(self, order, tail, ahead, lag):
+        count, body = len(order), len(order) - tail
         inner, outer = [], []
         for index in range(count + lag):
             first = [order[index + ahead]] if index + ahead < count else []
-            for slot in (2, 3, 1):
-                if index < count:
-                    begin = first if slot == 2 else []
-                    inner.append((begin, order[index], slot, slot > 1))
+            if index == body - 1:
+                first = order[index + ahead :]
+            elif index >= body:
+                first = []
+            if index < body:
+                inner.append((first, order[index], 2, True))
+                inner.append(([], order[index], 3, True))
+                inner.append(([], order[index], 1, False))
             if index < count:
                 outer.append((first, order[index], 1, False))
-            if index >= lag:
+            if lag <= index < body + lag:
                 outer.append(([], order[index - lag], 3, False))
                 outer.append(([], order[index - lag], 2, False))
+        last = order[body:]
+        for slot in (3, 1, 2):
+            inner += [([], unit, slot, slot > 1) for unit in last]
+        for slot in (2, 3):
+            outer += [([], unit, slot, False) for unit in last]
         self.waiting = list(zip(inner, outer))
+
+    def pump_until(self, left):
+        self.pump(max(0, len(self.waiting) - left))
 
     def pump(self, count):
         for _ in range(min(count, len(self.waiting))):
@@ -463,7 +484,7 @@
     w = Where()
     rows, group_rows, segments = sizes["rows"], sizes["group_rows"], sizes["segments"]
     depth, local_ch, half_ff = sizes["depth"], sizes["local_ch"], sizes["half_ff"]
-    width = out_all.shape[2]
+    width = out_all.shape[2] // SUMS
     mix_tiles, ffn_tiles = local_ch // LANES, half_ff // LANES
     member = w.member
 
@@ -496,16 +517,31 @@
     val_pieces = cut(val_weight, val_all, None, 2)
     gate_pieces = cut(gate_weight, gate_all, None, 2)
     out_pieces = cut(out_weight, out_all, None, 2)
-    up_gate_pieces = cut(up_gate_weight, up_gate_all, "columns", 2)
-    up_val_pieces = cut(up_val_weight, up_val_all, "columns", 2)
-    down_pieces = cut(down_weight, down_all, "rows", sizes["down_chunks"])
-    first = [val_pieces[0], gate_pieces[0], val_pieces[1], gate_pieces[1]]
-    later = [up_gate_pieces[0], up_val_pieces[0], up_gate_pieces[1], up_val_pieces[1]]
-    pieces = first + out_pieces + later + down_pieces
+    up_gate_pieces = cut(up_gate_weight, up_gate_all, "columns", UP_CUTS)
+    up_val_pieces = cut(up_val_weight, up_val_all, "columns", UP_CUTS)
+    down_rows = half_ff // 2
+    down_size = down_rows // 2
+    down_pieces = [
+        Piece(
+            down_weight,
+            down_all,
+            row * down_size,
+            down_size,
+            down_rows,
+            "rows",
+            None,
+            pl.ds(part * width, width),
+        )
+        for part in range(SUMS)
+        for row in range(2)
+    ]
+    mixed = [piece for pair in zip(val_pieces, gate_pieces) for piece in pair]
+    upward = [piece for pair in zip(up_gate_pieces, up_val_pieces) for piece in pair]
+    pieces = mixed + out_pieces + upward + down_pieces
     proj = list(range(0, 4))
     outs = list(range(4, 6))
-    ups = list(range(6, 10))
-    downs = list(range(10, 10 + len(down_pieces)))
+    ups = list(range(6, 6 + len(upward)))
+    downs = list(range(6 + len(upward), len(pieces)))
     stream = Stream(w, pieces, (z_send, z_recv, y_send, y_recv))
 
     def own_copy(index, source, held, sided):
@@ -555,12 +591,12 @@
 
     pl.semaphore_wait(barrier, len(friends) + w.inner.astype(jnp.int32))
 
-    ahead = 2
+    ahead = AHEAD
     for unit in range(ahead):
         stream.start(unit)
     mix_gather = RowGather(w, mix_rows, rows, group_rows, (mix_row_send, mix_row_recv))
     mix_gather.start(0)
-    stream.events(list(range(len(pieces))), ahead, 2)
+    stream.events(list(range(len(pieces))), len(downs), ahead, ahead)
     stream.pump(9)
     mix_gather.relay(0)
     stream.pump(8)
@@ -577,7 +613,7 @@
     for tile in range(mix_tiles):
         block = glu[:, tile * LANES : (tile + 1) * LANES].reshape(segments, LEN, LANES)
         glu_padded[tile * segments : (tile + 1) * segments, 32:, :] = block
-    stream.pump(1)
+    stream.pump(2)
 
     taps_count = conv_taps.shape[0]
     loads[2].wait()
@@ -593,6 +629,8 @@
                 shifted = glu_padded[tile * segments + segment, pl.ds(33 - taps_count + k, LEN), :]
                 total = total + shifted * taps[k : k + 1]
             conv_out[tile, rows_at(segment * LEN, LEN)] = total
+
+        stream.pump(1)
 
     sums = conv_out[0]
     squares = conv_out[0] * conv_out[0]
@@ -622,7 +660,7 @@
 
     for kind in (2, 1, 0):
         stat_copy(kind).start()
-    stream.pump(2)
+    stream.pump(3)
     for unit in outs:
         stream.arrive(unit)
     own_copies[2].wait()
@@ -643,14 +681,16 @@
         w,
         1,
         rows,
-        width,
+        width * SUMS,
         mix_part,
         (mix_send0, mix_send1),
         (mix_recv0, mix_recv1),
         (mix_sum_send, mix_sum_recv),
         result,
     )
-    places = [w.place, w.mate, w.source(3), w.source(2)]
+    places = [w.place]
+    for near, far in ((3, 1), (1, 2), (2, 3)):
+        places.append(jnp.where(w.inner, w.source(near), w.source(far)))
     for index in range(4 + 2):
         if index < 4:
             block = places[index]
@@ -659,8 +699,7 @@
             mix_sum.second(places[index - 1])
         if 2 <= index:
             mix_sum.third(places[index - 2])
-        if index % 2 == 1:
-            stream.pump(1)
+        stream.pump(1)
 
     loads[4].wait()
     loads[5].wait()
@@ -671,14 +710,14 @@
     ffn_gather = RowGather(w, ffn_rows, rows, group_rows, (ffn_row_send, ffn_row_recv))
     ffn_gather.start(0)
     ffn_gather.pair_copy().start()
-    stream.pump(1)
+    stream.pump(2)
     ffn_gather.relay(0)
-    stream.pump(2)
+    stream.pump(3)
     ffn_gather.pair_copy(incoming=True).wait_recv()
     ffn_gather.start(1)
-    stream.pump(2)
+    stream.pump(3)
     ffn_gather.relay(1)
-    stream.pump(6)
+    stream.pump_until(2 * len(downs))
     for unit in ups:
         stream.arrive(unit)
     own_copies[3].wait()
@@ -716,7 +755,6 @@
                 hidden[at, tile * LANES : (tile + 1) * LANES] = value.astype(BF16)
 
     feed(0)
-    stream.pump(1)
     feed(1)
     ffn_sum = RowScatter(
         w,
@@ -730,23 +768,33 @@
         result,
     )
     own_copies[5].wait()
-    slots = [None, 1, 3, 2]
-    stream.pump(1)
-    for index in range(4 + 2):
-        if index < 4:
-            block = places[index]
-            if index == 1:
-                stream.pump(len(stream.waiting))
+    blocks = [(index, part) for index in range(4) for part in range(SUMS)]
+    for step in range(len(blocks) + 2):
+        if step < len(blocks):
+            index, part = blocks[step]
+            if index == 3:
+                stream.pump_until(0)
+            else:
+                stream.pump(1)
             if index > 0:
-                for unit in downs:
-                    stream.y_copy(unit, slots[index], incoming=True).wait_recv()
-            ffn_sum.begin(block, product(hidden[...], down_all[block]))
-        if 1 <= index < 5:
-            ffn_sum.second(places[index - 1])
-        if 2 <= index:
-            ffn_sum.third(places[index - 2])
-    for index in (3, 2, 1, 0):
-        ffn_sum.fourth(places[3 - index])
+                for role, slots in enumerate(((0, 3, 1, 2), (0, 1, 2, 3))):
+                    chosen = jnp.logical_not(w.inner) if role else w.inner
+
+                    @pl.when(chosen)
+                    def _():
+                        for unit in downs[2 * part : 2 * part + 2]:
+                            stream.y_copy(unit, slots[index], incoming=True).wait_recv()
+
+            right = down_all[places[index], :, part * width : (part + 1) * width]
+            ffn_sum.begin(places[index] * SUMS + part, product(hidden[...], right))
+        if 1 <= step < len(blocks) + 1:
+            index, part = blocks[step - 1]
+            ffn_sum.second(places[index] * SUMS + part)
+        if 2 <= step:
+            index, part = blocks[step - 2]
+            ffn_sum.third(places[index] * SUMS + part)
+    for index, part in blocks:
+        ffn_sum.fourth(places[index] * SUMS + part)
     loads[7].wait()
     final = residual_ref[...].astype(F32) + rms_scale(result[...], gain_of(ffn_post_gain_in))
     out_staged[...] = final.astype(BF16)
@@ -762,8 +810,9 @@
     for kind in range(3):
         stat_copy(kind).wait_send()
     for index in range(4):
-        mix_sum.drain(places[index])
-        ffn_sum.drain(places[index])
+        mix_sum.drain(index)
+    for index in range(4 * SUMS):
+        ffn_sum.drain(index)
     leave.wait()
 
 
@@ -776,7 +825,6 @@
         "depth": 4 * val_weight.shape[0],
         "local_ch": val_weight.shape[1],
         "half_ff": up_gate_weight.shape[1] // 2,
-        "down_chunks": 4,
     }
 
 
@@ -804,7 +852,7 @@
     model = tokens.shape[1]
     mix_tiles, ffn_tiles = local_ch // LANES, half_ff // LANES
     padded_rows = -(-group_rows // LANES) * LANES
-    units = 10 + sizes["down_chunks"]
+    units = 6 + 2 * UP_CUTS + 2 * SUMS
     dma = pltpu.SemaphoreType.DMA
     shaped = [
         tokens,
@@ -848,17 +896,17 @@
         pltpu.VMEM((rows, model), BF16),
         pltpu.VMEM((rows, model), F32),
         pltpu.VMEM((4, 1, 2, 2, rows, width), F32),
-        pltpu.VMEM((4, 2, 2, 2, rows, width), F32),
+        pltpu.VMEM((4 * SUMS, 2, 2, 2, rows, width // SUMS), F32),
         pltpu.VMEM((4, 1, 2, rows, width), BF16),
         pltpu.VMEM((4, 1, rows, width), BF16),
         pltpu.VMEM((4, 1, 2, rows, width), BF16),
         pltpu.VMEM((4, 1, rows, width), BF16),
-        pltpu.VMEM((4, 2, 2, rows, width), BF16),
-        pltpu.VMEM((4, 2, rows, width), BF16),
-        pltpu.VMEM((4, rows, width), BF16),
-        pltpu.VMEM((4, 2, 2, rows, width), BF16),
-        pltpu.VMEM((4, 2, rows, width), BF16),
-        pltpu.VMEM((4, rows, width), BF16),
+        pltpu.VMEM((4 * SUMS, 2, 2, rows, width // SUMS), BF16),
+        pltpu.VMEM((4 * SUMS, 2, rows, width // SUMS), BF16),
+        pltpu.VMEM((4 * SUMS, rows, width // SUMS), BF16),
+        pltpu.VMEM((4 * SUMS, 2, 2, rows, width // SUMS), BF16),
+        pltpu.VMEM((4 * SUMS, 2, rows, width // SUMS), BF16),
+        pltpu.VMEM((4 * SUMS, rows, width // SUMS), BF16),
         pltpu.VMEM(tokens.shape, BF16),
         dma((9,)),
         dma((6,)),
@@ -874,8 +922,8 @@
         dma((3,)),
         dma((2, 4)),
         dma((2, 4)),
-        dma((3, 4)),
-        dma((3, 4)),
+        dma((3, 4 * SUMS)),
+        dma((3, 4 * SUMS)),
     ]
     return pl.pallas_call(
         functools.partial(layer_kernel, sizes),
@@ -899,10 +947,12 @@
     local_model = tokens.shape[1] // 4
     return (
         rows % 16 == 0
+        and local_model % (32 * UP_CUTS) == 0
+        and local_ff % 128 == 0
         and 4 * rows % LEN == 0
         and local_ch % LANES == 0
         and local_ff % (2 * LANES) == 0
-        and local_model % LANES == 0
+        and local_model % (SUMS * LANES) == 0
         and args[4].shape[0] <= 32
         and args[11].shape[1] <= 8
     )

time: 131 us -> 128 us (0.977)
  Pallas kernels: 129 us -> 127 us
    pallas_call x1, Pallas kernels: 129 us -> 127 us  [run_kernel(): pl.pallas_call(functools.partial(layer_kernel, sizes), out_shape=jax.Shap...]
where the time goes in v2:
time: 128 us
  Pallas kernels  127 us (99%)
  local copies, waits for them, and re-layouts  1.72 us (1%)
    pallas_call x1, Pallas kernels, run_kernel(): pl.pallas_call(functools.partial(layer_kernel, sizes), out_shape=jax.Shap...  127 us

profile of v2, /device:TPU:8, one launch (start us, length us, event | category | flops | bytes accessed | tf_op | source)
XLA Modules:
  0.0 128.3 jit_solution(12776504235458864622)
XLA Ops:
  0.0 126.6 %shard_map.136 = bf16[80,2048]{1,0:T(8,128)(2,1)} custom-call(bf16[80,2048]{1,0:T(8,128)(2,1)} %refs_0_.1, bf16[2048]{0:T(1024)(128)(2,1)} %refs_1_.1, bf16[512,256]{1,0:T(8,128)(2,1)} %refs_2_.1, bf16[512,256]{1,0:T(8,128)(2,1)} %refs_3_.1, bf16[31,1024]{1,0:T(8,128)(2,1)} %refs_4_.1, bf16[1024]{0:T(1024)(128)(2,1)} %refs_5_.1, bf16[256,512]{1,0:T(8,128)(2,1)} %refs_6_.1, ...), custom_call_target="tpu_custom_call" | custom-call | tf_op jit(solution)/shard_map/pallas_call | solution.py:928
  126.6 1.7 %copy.16 = bf16[80,2048]{1,0:T(8,128)(2,1)} copy(bf16[80,2048]{1,0:T(8,128)(2,1)} %shard_map.136) | data formatting | bytes 655360

commit v3 on v2

--- a/solution.py
+++ b/solution.py
@@ -585,15 +585,14 @@
     def gain_of(held):
         return held[...].astype(F32).reshape(1, held.shape[0])
 
+    pl.semaphore_wait(barrier, len(friends) + w.inner.astype(jnp.int32))
+
+    ahead = AHEAD
+    for unit in range(ahead):
+        stream.start(unit)
     loads[0].wait()
     loads[1].wait()
     mix_rows[own_rows] = rms_scale(tokens_in[...].astype(F32), gain_of(mix_gain_in)).astype(BF16)
-
-    pl.semaphore_wait(barrier, len(friends) + w.inner.astype(jnp.int32))
-
-    ahead = AHEAD
-    for unit in range(ahead):
-        stream.start(unit)
     mix_gather = RowGather(w, mix_rows, rows, group_rows, (mix_row_send, mix_row_recv))
     mix_gather.start(0)
     stream.events(list(range(len(pieces))), len(downs), ahead, ahead)

time: 128 us -> 128 us (level)
  no operation moved by 1% of the time
where the time goes in v3:
time: 128 us
  Pallas kernels  127 us (99%)
  local copies, waits for them, and re-layouts  1.72 us (1%)
    pallas_call x1, Pallas kernels, run_kernel(): pl.pallas_call(functools.partial(layer_kernel, sizes), out_shape=jax.Shap...  127 us

profile of v3, /device:TPU:8, one launch (start us, length us, event | category | flops | bytes accessed | tf_op | source)
XLA Modules:
  0.0 128.3 jit_solution(13867123788514224877)
XLA Ops:
  0.0 126.6 %shard_map.136 = bf16[80,2048]{1,0:T(8,128)(2,1)} custom-call(bf16[80,2048]{1,0:T(8,128)(2,1)} %refs_0_.1, bf16[2048]{0:T(1024)(128)(2,1)} %refs_1_.1, bf16[512,256]{1,0:T(8,128)(2,1)} %refs_2_.1, bf16[512,256]{1,0:T(8,128)(2,1)} %refs_3_.1, bf16[31,1024]{1,0:T(8,128)(2,1)} %refs_4_.1, bf16[1024]{0:T(1024)(128)(2,1)} %refs_5_.1, bf16[256,512]{1,0:T(8,128)(2,1)} %refs_6_.1, ...), custom_call_target="tpu_custom_call" | custom-call | tf_op jit(solution)/shard_map/pallas_call | solution.py:927
  126.6 1.7 %copy.16 = bf16[80,2048]{1,0:T(8,128)(2,1)} copy(bf16[80,2048]{1,0:T(8,128)(2,1)} %shard_map.136) | data formatting | bytes 655360
